TPU v7x, 32 devices: a whole 2x2x4 slice. The times are simulated.
32 devices in a mesh: sp: 4 (over y, x), dp: 8 (over z, core).
Axes of the slice: x: 2, y: 2, z: 4, core: 2. Of those that a mesh axis runs over, the one named last changes fastest.
Arguments:
- value_half: bfloat16 [8, 1024, 2048], P('dp', 'sp'), may hold values from -6 to 6
- gate_half: bfloat16 [8, 1024, 2048], P('dp', 'sp'), may hold values from -6 to 6
- upstream: bfloat16 [8, 1024, 2048], P('dp', 'sp'), may hold values from -6 to 6
- conv_taps: float32 [31, 2048], P(None, 'sp'), may hold values from -1 to 1
- norm_gain: float32 [2048], replicated, may hold values from 0.1 to 1.9
- out_weight: bfloat16 [2048, 2048], P('dp'), may hold values from -0.125 to 0.125
Outputs:
- grad_value: bfloat16 [8, 1024, 2048], P('dp', 'sp')
- grad_gate: bfloat16 [8, 1024, 2048], P('dp', 'sp')
- grad_taps: float32 [31, 2048], P(None, 'sp')
- grad_gain: float32 [2048], replicated
- grad_weight: float32 [2048, 2048], P('dp')
All inputs are finite; a program needn't handle non-finite values.
Results may differ from a plain program's by a relative error of at most 0.0062.
Values may be sent and summed in bfloat16 or wider, within the bound.
A program may use at most 128 MiB of HBM per device.

v0:
```python
import jax
import jax.numpy as jnp
from jax import lax
from jax.sharding import PartitionSpec as P

NORM_EPS = 1e-05


def body(value_half, gate_half, upstream, conv_taps, norm_gain, out_weight):
    tap_count = conv_taps.shape[0]
    sig_gate = jax.nn.sigmoid(gate_half.astype(jnp.float32))
    value_wide = value_half.astype(jnp.float32)
    glu = (value_wide * sig_gate).astype(jnp.bfloat16)
    glu_heads = lax.all_to_all(glu, "sp", split_axis=2, concat_axis=1, tiled=True).astype(
        jnp.float32
    )
    length = glu_heads.shape[1]
    padded = jnp.pad(glu_heads, ((0, 0), (tap_count - 1, 0), (0, 0)))
    conv_out = jnp.zeros_like(glu_heads)
    for offset in range(tap_count):
        conv_out = conv_out + conv_taps[offset] * padded[:, offset : offset + length]
    conv_tokens = lax.all_to_all(
        conv_out.astype(jnp.bfloat16), "sp", split_axis=1, concat_axis=2, tiled=True
    ).astype(jnp.float32)
    row_mean = jnp.mean(conv_tokens, axis=-1, keepdims=True)
    centered = conv_tokens - row_mean
    inv_scale = lax.rsqrt(jnp.mean(centered * centered, axis=-1, keepdims=True) + NORM_EPS)
    normed = centered * inv_scale
    scaled = normed * norm_gain
    sig_scaled = jax.nn.sigmoid(scaled)
    activated = (scaled * sig_scaled).astype(jnp.bfloat16)[0]
    upstream_rows = upstream[0]
    columns = upstream_rows
    grad_act = jnp.dot(
        columns,
        lax.all_gather(out_weight, "dp", axis=0, tiled=True),
        preferred_element_type=jnp.float32,
    )
    grad_scaled = grad_act[None] * sig_scaled * (1.0 + scaled * (1.0 - sig_scaled))
    gain_part = jnp.sum(grad_scaled * normed, axis=(0, 1))
    grad_normed = grad_scaled * norm_gain
    grad_conv_out = inv_scale * (
        grad_normed
        - jnp.mean(grad_normed, axis=-1, keepdims=True)
        - normed * jnp.mean(grad_normed * normed, axis=-1, keepdims=True)
    )
    grad_heads = lax.all_to_all(
        grad_conv_out.astype(jnp.bfloat16), "sp", split_axis=2, concat_axis=1, tiled=True
    ).astype(jnp.float32)
    grad_padded = jnp.pad(grad_heads, ((0, 0), (0, tap_count - 1), (0, 0)))
    grad_glu = jnp.zeros_like(grad_heads)
    tap_terms = []
    for offset in range(tap_count):
        first = tap_count - 1 - offset
        grad_glu = grad_glu + conv_taps[offset] * grad_padded[:, first : first + length]
        tap_terms.append(jnp.sum(grad_heads * padded[:, offset : offset + length], axis=(0, 1)))
    grad_taps = lax.psum(jnp.stack(tap_terms), "dp")
    grad_tokens = lax.all_to_all(
        grad_glu.astype(jnp.bfloat16), "sp", split_axis=1, concat_axis=2, tiled=True
    ).astype(jnp.float32)
    grad_value = (grad_tokens * sig_gate).astype(jnp.bfloat16)
    grad_gate = (grad_tokens * value_wide * sig_gate * (1.0 - sig_gate)).astype(jnp.bfloat16)
    grad_gain = lax.psum(gain_part, ("sp", "dp"))
    columns = upstream_rows
    owned = lax.psum_scatter(
        lax.dot_general(
            columns, activated, (((0,), (0,)), ((), ())), preferred_element_type=jnp.float32
        ),
        "dp",
        scatter_dimension=0,
        tiled=True,
    )
    grad_weight = lax.psum(owned, "sp")
    return (grad_value, grad_gate, grad_taps, grad_gain, grad_weight)


def solution(mesh):
    placed = (
        P("dp", "sp", None),
        P("dp", "sp", None),
        P("dp", "sp", None),
        P(None, "sp"),
        P(),
        P("dp", None),
    )
    return jax.shard_map(
        body,
        mesh=mesh,
        in_specs=placed,
        out_specs=(P("dp", "sp", None), P("dp", "sp", None), P(None, "sp"), P(), P("dp", None)),
        check_vma=False,
    )
```

profile of v0, /device:TPU:0, one launch (start us, length us, event | category | flops | bytes accessed | tf_op | source)
XLA Modules:
  0.0 395.5 jit_solution(13518251392995277205)
XLA Ops:
  7.2 0.0 all-gather.2.cloned.1.call-start
  7.2 0.7 all-gather.2.cloned.1.call-update
  7.9 1.5 copy.56
  9.4 1.9 copy.57
  11.3 0.6 fusion.1
  11.9 12.9 %copy.90 = bf16[1,256,2048]{1,0,2:T(2,128)(2,1)} copy(bf16[1,256,2048]{1,2,0:T(8,128)(2,1)S(1)} %fusion.1) | data formatting | bytes 2097152 | tf_op jit(solution)/shard_map/convert_element_type | solution.py:13
  24.8 0.5 broadcast.201
  25.3 11.6 %reduce.17 = bf16[2048,256]{1,0:T(8,128)(2,1)S(1)} reduce(bf16[2048,1,256]{2,1,0:T(2,128)(2,1)} %bitcast.178, bf16[]{:T(256)} %broadcast.201), dimensions={1}, to_apply=%bitcast.161.reduce_sub_computation | reduce | bytes 2097154
  37.0 1.6 reshape.389
  38.6 5.4 %all-to-all-start = ((bf16[4,2,65536]{2,1,0:T(2,128)(2,1)}), bf16[4,2,65536]{2,1,0:T(2,128)(2,1)}, u32[]{:S(2)}, u32[]{:S(2)}) async-start(bf16[4,2,65536]{2,1,0:T(2,128)(2,1)} %reshape.389), calls=%async_computation | async-start | bytes 2097152 | tf_op jit(solution)/shard_map/all_to_all | solution.py:14
  44.1 14.2 %all-to-all-done = bf16[4,2,65536]{2,1,0:T(2,128)(2,1)} async-done(((bf16[4,2,65536]{2,1,0:T(2,128)(2,1)}), bf16[4,2,65536]{2,1,0:T(2,128)(2,1)}, u32[]{:S(2)}, u32[]{:S(2)}) %all-to-all-start) | async-done | bytes 1048608 | tf_op jit(solution)/shard_map/all_to_all | solution.py:14
  58.3 2.6 reshape.390
  60.9 1.6 copy_convert_fusion.2
  62.5 0.5 copy-done.3
  63.0 1.9 copy.60
  64.9 8.0 %add_convert_fusion.1 = bf16[1,1024,512]{2,1,0:T(8,128)(2,1)S(1)} fusion(f32[1,1024,512]{2,1,0:T(8,128)S(1)} %bitcast.163, f32[512]{0:T(512)S(1)} %bitcast.207, f32[512]{0:T(512)S(1)} %bitcast.209, f32[512]{0:T(512)S(1)} %bitcast.213, f32[512]{0:T(512)S(1)} %bitcast.215, f32[512]{0:T(512)S(1)} %bitcast.217, f32[512]{0:T(512)S(1)} %bitcast.219, ...), kind=kLoop, calls=%fused_computation.88 | loop fusion | flops 32505856 | bytes 3209216 | tf_op jit(solution)/shard_map/convert_element_type | solution.py:23
  72.9 2.9 copy.89
  75.8 8.1 %reduce.18 = bf16[1024,512]{1,0:T(8,128)(2,1)S(1)} reduce(bf16[1024,1,512]{2,1,0:T(2,128)(2,1)} %bitcast.180, bf16[]{:T(256)} %broadcast.201), dimensions={1}, to_apply=%bitcast.160.reduce_sub_computation | reduce | bytes 2097154
  83.9 2.0 reshape.391
  85.9 4.3 %all-to-all-start.1 = ((bf16[4,2,65536]{2,1,0:T(2,128)(2,1)}), bf16[4,2,65536]{2,1,0:T(2,128)(2,1)}, u32[]{:S(2)}, u32[]{:S(2)}) async-start(bf16[4,2,65536]{2,1,0:T(2,128)(2,1)} %reshape.391), calls=%async_computation.1 | async-start | bytes 2097152 | tf_op jit(solution)/shard_map/all_to_all | solution.py:22
  90.2 0.0 reduce-scatter.2.cloned.1.call-start
  90.2 13.4 %all-to-all-done.1 = bf16[4,2,65536]{2,1,0:T(2,128)(2,1)} async-done(((bf16[4,2,65536]{2,1,0:T(2,128)(2,1)}), bf16[4,2,65536]{2,1,0:T(2,128)(2,1)}, u32[]{:S(2)}, u32[]{:S(2)}) %all-to-all-start.1) | async-done | bytes 1048608 | tf_op jit(solution)/shard_map/all_to_all | solution.py:22
  103.6 3.0 reshape.392
  106.6 0.2 fusion.36
  106.9 1.1 copy-done.5
  108.0 1.8 copy_convert_fusion.1
  109.8 1.8 copy.63
  111.6 1.9 fusion.10
  113.5 1.8 fusion.32
  115.4 2.3 copy.71
  117.6 9.3 %convolution_bitcast_fusion = f32[2048,2048]{0,1:T(8,128)} fusion(bf16[256,2048]{0,1:T(8,128)(2,1)} %bitcast.186, bf16[1,256,2048]{2,1,0:T(8,128)(2,1)S(1)} %copy-done), kind=kOutput, calls=%fused_computation | convolution fusion | flops 2147483648 | bytes 18874368 | tf_op jit(solution)/shard_map/dot_general | solution.py:66
  126.9 1.4 copy.64
  128.3 0.9 copy.75
  129.2 5.7 %multiply_reduce_fusion = (f32[2048]{0:T(1024)S(1)}, f32[256]{0:T(256)S(1)}, f32[256]{0:T(256)S(1)}, f32[256,2048]{1,0:T(8,128)S(1)}) fusion(f32[256,2048]{1,0:T(8,128)S(1)} %bitcast.176, f32[256]{0:T(256)S(1)} %broadcast_multiply_fusion.2, f32[256]{0:T(256)S(1)} %add_rsqrt_fusion, f32[2048]{0:T(1024)S(1)} %copy-done.11, ...), kind=kOutput, calls=%fused_computation.20 | convolution fusion | flops 2156393984 | bytes 13651968 | tf_op jit(solution)/shard_map/dot_general | solution.py:34
  135.0 0.7 fusion.33
  135.7 1.7 copy.65
  137.4 10.8 %reduce.19 = bf16[2048,256]{1,0:T(8,128)(2,1)S(1)} reduce(bf16[2048,1,256]{2,1,0:T(2,128)(2,1)S(1)} %bitcast.182, bf16[]{:T(256)} %broadcast.201), dimensions={1}, to_apply=%bitcast.148.reduce_sub_computation | reduce | bytes 2097154
  148.1 1.6 reshape.393
  149.8 3.5 all-to-all-start.2
  153.3 0.0 all-reduce.4.cloned.1.call-start
  153.4 48.8 %psum.22 = f32[2048]{0:T(1024)} all-reduce(f32[2048]{0:T(1024)S(1)} %get-tuple-element.35), channel_id=1, replica_groups=mesh['sp'=4,'dp'=8] {'sp','dp'}, use_global_device_ids=true, to_apply=%region_39.40 | all-reduce | flops 2048 | bytes 16384 | tf_op jit(solution)/shard_map/psum | solution.py:63
  202.1 1.0 reshape.394
  203.1 1.6 copy_convert_fusion
  204.7 0.5 copy-done.4
  205.1 1.9 copy.67
  207.1 8.0 %add_convert_fusion = bf16[1,1024,512]{2,1,0:T(8,128)(2,1)S(1)} fusion(f32[1,1024,512]{2,1,0:T(8,128)S(1)} %bitcast.162, f32[512]{0:T(512)S(1)} %bitcast.208, f32[512]{0:T(512)S(1)} %bitcast.210, f32[512]{0:T(512)S(1)} %bitcast.214, f32[512]{0:T(512)S(1)} %bitcast.216, f32[512]{0:T(512)S(1)} %bitcast.218, f32[512]{0:T(512)S(1)} %bitcast.220, ...), kind=kLoop, calls=%fused_computation.52 | loop fusion | flops 32505856 | bytes 3209216 | tf_op jit(solution)/shard_map/convert_element_type | solution.py:59
  215.0 81.4 %reduce-scatter.2.cloned.1.call-done = f32[256,2048]{0,1:T(8,128)} async-done(((f32[2048,2048]{0,1:T(8,128)}), f32[256,2048]{0,1:T(8,128)}) %reduce-scatter.2.cloned.1.call-update) | async-done | bytes 2097168 | tf_op jit(solution)/shard_map/reduce_scatter | solution.py:65
  296.5 17.9 %multiply_reduce_fusion.2 = (f32[512]{0:T(512)S(1)}, f32[512]{0:T(512)S(1)}, f32[512]{0:T(512)S(1)}, f32[512]{0:T(512)S(1)}, f32[512]{0:T(512)S(1)}, /*index=5*/...) fusion(f32[1,1024,512]{2,1,0:T(8,128)} %bitcast.164, ...), kind=kLoop, calls=%fused_computation.22 | loop fusion | flops 18865152 | bytes 4231168 | tf_op jit(solution)/shard_map/reduce_sum | solution.py:56
  314.4 2.9 copy.88
  317.4 8.0 %reduce.20 = bf16[1024,512]{1,0:T(8,128)(2,1)S(1)} reduce(bf16[1024,1,512]{2,1,0:T(2,128)(2,1)} %bitcast.179, bf16[]{:T(256)} %broadcast.201), dimensions={1}, to_apply=%bitcast.159.reduce_sub_computation | reduce | bytes 2097154
  325.4 2.0 reshape.395
  327.4 3.7 all-to-all-start.3
  331.1 2.6 multiply_reduce_fusion.1
  333.7 11.8 %multiply_reduce_fusion.3 = (f32[512]{0:T(512)S(1)}, f32[512]{0:T(512)S(1)}, f32[512]{0:T(512)S(1)}, f32[512]{0:T(512)S(1)}, f32[512]{0:T(512)S(1)}, /*index=5*/...) fusion(f32[1,1024,512]{2,1,0:T(8,128)} %bitcast.165, ...), kind=kLoop, calls=%fused_computation.23 | loop fusion | flops 12576768 | bytes 4218880 | tf_op jit(solution)/shard_map/reduce_sum | solution.py:56
  345.5 0.1 stack.127
  345.7 27.2 %psum.21 = f32[31,512]{1,0:T(8,128)} all-reduce(f32[31,512]{1,0:T(8,128)S(1)} %stack.127), channel_id=1, replica_groups=mesh['sp'=4,'dp'=8] {'dp'}, use_global_device_ids=true, to_apply=%region_37.38 | all-reduce | flops 15872 | bytes 126976 | tf_op jit(solution)/shard_map/psum | solution.py:57
  372.9 0.9 reshape.396
  373.8 0.3 copy.69
  374.1 1.6 convert_bitcast_fusion
  375.7 3.0 copy.70
  378.8 3.4 fusion.4
  382.1 2.3 copy.72
  384.4 1.4 copy.73
  385.8 2.9 copy.74
  (37 shorter events, 0.3 us)
Async XLA Ops:
  7.2 110.5 %copy-start = (bf16[1,256,2048]{2,1,0:T(8,128)(2,1)S(1)}, bf16[1,256,2048]{2,1,0:T(8,128)(2,1)}, u32[]{:S(2)}) copy-start(bf16[1,256,2048]{2,1,0:T(8,128)(2,1)} %param.8) | copy-start | bytes 3145732
  7.2 122.0 %all-gather.2.cloned.1.call-start = ((), (), s32[]{:S(2)}) async-start(), calls=%async_computation.5 | async-start | bytes 9437184 | tf_op jit(solution)/shard_map/all_gather | solution.py:36
  9.4 2.5 copy-start.6
  11.3 13.5 %copy-start.8 = (bf16[1,256,2048]{1,2,0:T(8,128)(2,1)}, bf16[1,256,2048]{1,2,0:T(8,128)(2,1)S(1)}, u32[]{:S(2)}) copy-start(bf16[1,256,2048]{1,2,0:T(8,128)(2,1)S(1)} %copy.57) | copy-start | bytes 3145732
  37.0 7.1 %copy-start.10 = (f32[31,512]{1,0:T(8,128)S(1)}, f32[31,512]{1,0:T(8,128)}, u32[]{:S(2)}) copy-start(f32[31,512]{1,0:T(8,128)} %param.9) | copy-start | bytes 190468
  38.6 19.7 %all-to-all-start = ((bf16[4,2,65536]{2,1,0:T(2,128)(2,1)}), bf16[4,2,65536]{2,1,0:T(2,128)(2,1)}, u32[]{:S(2)}, u32[]{:S(2)}) async-start(bf16[4,2,65536]{2,1,0:T(2,128)(2,1)} %reshape.389), calls=%async_computation | async-start | bytes 2097152 | tf_op jit(solution)/shard_map/all_to_all | solution.py:14
  60.9 2.0 copy-start.3
  64.9 10.9 %copy-start.2 = (f32[1,4,256,512]{3,2,1,0:T(8,128)}, f32[1,4,256,512]{3,2,1,0:T(8,128)S(1)}, u32[]{:S(2)}) copy-start(f32[1,4,256,512]{3,2,1,0:T(8,128)S(1)} %copy.60) | copy-start | bytes 6291460
  83.9 6.3 %copy-start.11 = (f32[2048]{0:T(1024)S(1)}, f32[2048]{0:T(1024)}, u32[]{:S(2)}) copy-start(f32[2048]{0:T(1024)} %param.10) | copy-start | bytes 24580
  85.9 17.7 %all-to-all-start.1 = ((bf16[4,2,65536]{2,1,0:T(2,128)(2,1)}), bf16[4,2,65536]{2,1,0:T(2,128)(2,1)}, u32[]{:S(2)}, u32[]{:S(2)}) async-start(bf16[4,2,65536]{2,1,0:T(2,128)(2,1)} %reshape.391), calls=%async_computation.1 | async-start | bytes 2097152 | tf_op jit(solution)/shard_map/all_to_all | solution.py:22
  90.2 206.3 %reduce-scatter.2.cloned.1.call-start = ((), (), s32[]{:S(2)}) async-start(), calls=%async_computation.6 | async-start | bytes 18874368 | tf_op jit(solution)/shard_map/reduce_scatter | solution.py:65
  106.6 1.3 copy-start.5
  149.8 52.3 %all-to-all-start.2 = ((bf16[4,2,65536]{2,1,0:T(2,128)(2,1)}), bf16[4,2,65536]{2,1,0:T(2,128)(2,1)S(1)}, u32[]{:S(2)}, u32[]{:S(2)}) async-start(bf16[4,2,65536]{2,1,0:T(2,128)(2,1)} %reshape.393), calls=%async_computation.2 | async-start | bytes 2097152 | tf_op jit(solution)/shard_map/all_to_all | solution.py:47
  153.3 232.5 %all-reduce.4.cloned.1.call-start = ((), (), s32[]{:S(2)}) async-start(), calls=%async_computation.7 | async-start | bytes 4194304 | tf_op jit(solution)/shard_map/psum | solution.py:73
  203.1 2.0 copy-start.4
  327.4 45.5 %all-to-all-start.3 = ((bf16[4,2,65536]{2,1,0:T(2,128)(2,1)}), bf16[4,2,65536]{2,1,0:T(2,128)(2,1)S(1)}, u32[]{:S(2)}, u32[]{:S(2)}) async-start(bf16[4,2,65536]{2,1,0:T(2,128)(2,1)} %reshape.395), calls=%async_computation.3 | async-start | bytes 2097152 | tf_op jit(solution)/shard_map/all_to_all | solution.py:58
  375.7 3.0 copy-start.7
  375.7 3.0 copy-start.9
  384.4 4.3 %copy-start.1 = (bf16[1,256,2048]{2,1,0:T(8,128)(2,1)S(1)}, bf16[1,256,2048]{2,1,0:T(8,128)(2,1)}, u32[]{:S(2)}) copy-start(bf16[1,256,2048]{2,1,0:T(8,128)(2,1)} %param.8) | copy-start | bytes 3145732
Sparse Core Ops, SparseCore 0:
  9.6 84.7 all-gather.1
  127.1 169.3 reduce-scatter.1
  299.6 69.1 all-reduce.3
where the time goes:
time: 402 us; the launch traced here: 395 us
  waiting for transfers between devices  110 us (27%)
  other arithmetic  102 us (25%)
  blocking collectives  75.9 us (19%)
  local copies, waits for them, and re-layouts  61.5 us (15%)
  starting transfers between devices  16.9 us (4%)
  matrix products  15 us (4%)
  between operations  14.3 us (4%)
    reduce_scatter x1, waiting for transfers between devices, body(): lax.psum_scatter(lax.dot_general(columns, activated, (((0,), (0,)), ((),...  81.4 us
    psum x1, blocking collectives, body(): grad_gain = lax.psum(gain_part, ('sp', 'dp'))  48.8 us
    unnamed x4, other arithmetic  38.5 us
    reduce_sum x4, other arithmetic, body(): jnp.sum(grad_heads * padded[:, offset:offset + length], axis=(0, 1))  32.4 us
    unnamed x39, local copies, waits for them, and re-layouts  28.2 us
    psum x1, blocking collectives, body(): grad_taps = lax.psum(jnp.stack(tap_terms), 'dp')  27.2 us
    all_to_all x1, waiting for transfers between devices, body(): lax.all_to_all(glu, 'sp', split_axis=2, concat_axis=1, tiled=True)  14.2 us
    all_to_all x1, waiting for transfers between devices, body(): lax.all_to_all(conv_out.astype(jnp.bfloat16), 'sp', split_axis=1, concat_...  13.4 us
  transfers between devices with their start and end apart: 7, of which 3 were waited for; matrix products, arithmetic and copies ran while one was open for 44% of the time, Pallas kernels for 0%

commit v1 on v0

--- a/solution.py
+++ b/solution.py
@@ -54,7 +54,7 @@
         first = tap_count - 1 - offset
         grad_glu = grad_glu + conv_taps[offset] * grad_padded[:, first : first + length]
         tap_terms.append(jnp.sum(grad_heads * padded[:, offset : offset + length], axis=(0, 1)))
-    grad_taps = lax.psum(jnp.stack(tap_terms), "dp")
+    grad_taps = jnp.sum(lax.all_gather(jnp.stack(tap_terms), "dp"), axis=0)
     grad_tokens = lax.all_to_all(
         grad_glu.astype(jnp.bfloat16), "sp", split_axis=1, concat_axis=2, tiled=True
     ).astype(jnp.float32)

time: 402 us -> 383 us (0.953)
  blocking collectives: 75.9 us -> 63.6 us
  waiting for transfers between devices: 110 us -> 102 us
    reduce_scatter x1, waiting for transfers between devices: 81.4 us -> 46.1 us  [body(): lax.psum_scatter(lax.dot_general(columns, activated, (((0,), (0,)), ((),...]
    psum x1, waiting for transfers between devices: 0.01 us -> 28 us  [body(): grad_weight = lax.psum(owned, 'sp')]
    psum x1 -> x0, blocking collectives: 27.2 us -> none  [body(): grad_taps = lax.psum(jnp.stack(tap_terms), 'dp')]
    all_gather x0 -> x1, blocking collectives: none -> 14.8 us  [body(): grad_taps = jnp.sum(lax.all_gather(jnp.stack(tap_terms), 'dp'), axis=0)]
  transfers between devices with their start and end apart: 7 -> 7, of which waited for: 3 -> 4; matrix products, arithmetic and copies ran while one was open for 44% -> 46% of each run, Pallas kernels for 0% -> 0%
where the time goes in v1:
time: 383 us; the launch traced here: 377 us
  other arithmetic  103 us (27%)
  waiting for transfers between devices  102 us (27%)
  blocking collectives  63.6 us (17%)
  local copies, waits for them, and re-layouts  61.3 us (16%)
  starting transfers between devices  17.5 us (5%)
  matrix products  15 us (4%)
  between operations  14.3 us (4%)
    psum x1, blocking collectives, body(): grad_gain = lax.psum(gain_part, ('sp', 'dp'))  48.8 us
    reduce_scatter x1, waiting for transfers between devices, body(): lax.psum_scatter(lax.dot_general(columns, activated, (((0,), (0,)), ((),...  46.1 us
    unnamed x4, other arithmetic  38.8 us
    reduce_sum x4, other arithmetic, body(): jnp.sum(grad_heads * padded[:, offset:offset + length], axis=(0, 1))  32.3 us
    unnamed x39, local copies, waits for them, and re-layouts  28 us
    psum x1, waiting for transfers between devices, body(): grad_weight = lax.psum(owned, 'sp')  28 us
    all_gather x1, blocking collectives, body(): grad_taps = jnp.sum(lax.all_gather(jnp.stack(tap_terms), 'dp'), axis=0)  14.8 us
    all_to_all x1, waiting for transfers between devices, body(): lax.all_to_all(glu, 'sp', split_axis=2, concat_axis=1, tiled=True)  14.2 us
  transfers between devices with their start and end apart: 7, of which 4 were waited for; matrix products, arithmetic and copies ran while one was open for 46% of the time, Pallas kernels for 0%

profile of v1, /device:TPU:0, one launch (start us, length us, event | category | flops | bytes accessed | tf_op | source)
XLA Modules:
  0.0 377.0 jit_solution(1680223140808094618)
XLA Ops:
  7.2 0.7 all-gather.4.cloned.1.call-update
  7.9 1.5 copy.56
  9.4 1.9 copy.57
  11.3 0.6 fusion.1
  11.9 12.9 %copy.90 = bf16[1,256,2048]{1,0,2:T(2,128)(2,1)} copy(bf16[1,256,2048]{1,2,0:T(8,128)(2,1)S(1)} %fusion.1) | data formatting | bytes 2097152 | tf_op jit(solution)/shard_map/convert_element_type | solution.py:13
  24.8 0.5 broadcast.201
  25.3 11.6 %reduce.18 = bf16[2048,256]{1,0:T(8,128)(2,1)S(1)} reduce(bf16[2048,1,256]{2,1,0:T(2,128)(2,1)} %bitcast.179, bf16[]{:T(256)} %broadcast.201), dimensions={1}, to_apply=%bitcast.162.reduce_sub_computation | reduce | bytes 2097154
  37.0 1.6 reshape.393
  38.6 5.4 %all-to-all-start = ((bf16[4,2,65536]{2,1,0:T(2,128)(2,1)}), bf16[4,2,65536]{2,1,0:T(2,128)(2,1)}, u32[]{:S(2)}, u32[]{:S(2)}) async-start(bf16[4,2,65536]{2,1,0:T(2,128)(2,1)} %reshape.393), calls=%async_computation | async-start | bytes 2097152 | tf_op jit(solution)/shard_map/all_to_all | solution.py:14
  44.1 14.2 %all-to-all-done = bf16[4,2,65536]{2,1,0:T(2,128)(2,1)} async-done(((bf16[4,2,65536]{2,1,0:T(2,128)(2,1)}), bf16[4,2,65536]{2,1,0:T(2,128)(2,1)}, u32[]{:S(2)}, u32[]{:S(2)}) %all-to-all-start) | async-done | bytes 1048608 | tf_op jit(solution)/shard_map/all_to_all | solution.py:14
  58.3 2.6 reshape.394
  60.9 1.6 copy_convert_fusion.2
  62.5 0.5 copy-done.3
  63.0 1.9 copy.60
  64.9 8.0 %add_convert_fusion.1 = bf16[1,1024,512]{2,1,0:T(8,128)(2,1)S(1)} fusion(f32[1,1024,512]{2,1,0:T(8,128)S(1)} %bitcast.164, f32[512]{0:T(512)S(1)} %bitcast.209, f32[512]{0:T(512)S(1)} %bitcast.211, f32[512]{0:T(512)S(1)} %bitcast.215, f32[512]{0:T(512)S(1)} %bitcast.217, f32[512]{0:T(512)S(1)} %bitcast.219, f32[512]{0:T(512)S(1)} %bitcast.221, ...), kind=kLoop, calls=%fused_computation.88 | loop fusion | flops 32505856 | bytes 3209216 | tf_op jit(solution)/shard_map/convert_element_type | solution.py:23
  72.9 2.9 copy.89
  75.8 8.1 %reduce.19 = bf16[1024,512]{1,0:T(8,128)(2,1)S(1)} reduce(bf16[1024,1,512]{2,1,0:T(2,128)(2,1)} %bitcast.181, bf16[]{:T(256)} %broadcast.201), dimensions={1}, to_apply=%bitcast.161.reduce_sub_computation | reduce | bytes 2097154
  83.9 2.0 reshape.395
  85.9 4.3 %all-to-all-start.1 = ((bf16[4,2,65536]{2,1,0:T(2,128)(2,1)}), bf16[4,2,65536]{2,1,0:T(2,128)(2,1)}, u32[]{:S(2)}, u32[]{:S(2)}) async-start(bf16[4,2,65536]{2,1,0:T(2,128)(2,1)} %reshape.395), calls=%async_computation.1 | async-start | bytes 2097152 | tf_op jit(solution)/shard_map/all_to_all | solution.py:22
  90.2 13.4 %all-to-all-done.1 = bf16[4,2,65536]{2,1,0:T(2,128)(2,1)} async-done(((bf16[4,2,65536]{2,1,0:T(2,128)(2,1)}), bf16[4,2,65536]{2,1,0:T(2,128)(2,1)}, u32[]{:S(2)}, u32[]{:S(2)}) %all-to-all-start.1) | async-done | bytes 1048608 | tf_op jit(solution)/shard_map/all_to_all | solution.py:22
  103.6 2.8 reshape.396
  106.4 0.2 fusion.36
  106.7 1.1 copy-done.5
  107.8 1.8 copy_convert_fusion.1
  109.6 1.8 copy.63
  111.4 1.9 fusion.10
  113.3 1.8 fusion.32
  115.2 2.3 copy.71
  117.4 9.3 %convolution_bitcast_fusion = f32[2048,2048]{0,1:T(8,128)} fusion(bf16[256,2048]{0,1:T(8,128)(2,1)} %bitcast.187, bf16[1,256,2048]{2,1,0:T(8,128)(2,1)S(1)} %copy-done), kind=kOutput, calls=%fused_computation | convolution fusion | flops 2147483648 | bytes 18874368 | tf_op jit(solution)/shard_map/dot_general | solution.py:66
  126.7 1.4 copy.64
  128.1 0.9 copy.75
  129.0 5.8 %multiply_reduce_fusion = (f32[2048]{0:T(1024)S(1)}, f32[256]{0:T(256)S(1)}, f32[256]{0:T(256)S(1)}, f32[256,2048]{1,0:T(8,128)S(1)}) fusion(f32[256,2048]{1,0:T(8,128)S(1)} %bitcast.177, f32[256]{0:T(256)S(1)} %broadcast_multiply_fusion.2, f32[256]{0:T(256)S(1)} %add_rsqrt_fusion, f32[2048]{0:T(1024)S(1)} %copy-done.11, ...), kind=kOutput, calls=%fused_computation.20 | convolution fusion | flops 2156393984 | bytes 13651968 | tf_op jit(solution)/shard_map/dot_general | solution.py:34
  134.8 0.7 fusion.33
  135.5 1.7 copy.65
  137.2 11.0 %reduce.20 = bf16[2048,256]{1,0:T(8,128)(2,1)S(1)} reduce(bf16[2048,1,256]{2,1,0:T(2,128)(2,1)S(1)} %bitcast.183, bf16[]{:T(256)} %broadcast.201), dimensions={1}, to_apply=%bitcast.149.reduce_sub_computation | reduce | bytes 2097154
  148.2 1.6 reshape.397
  149.8 3.5 all-to-all-start.2
  153.4 48.8 %psum.14 = f32[2048]{0:T(1024)} all-reduce(f32[2048]{0:T(1024)S(1)} %get-tuple-element.35), channel_id=1, replica_groups=mesh['sp'=4,'dp'=8] {'sp','dp'}, use_global_device_ids=true, to_apply=%region_39.40 | all-reduce | flops 2048 | bytes 16384 | tf_op jit(solution)/shard_map/psum | solution.py:63
  202.2 1.0 reshape.398
  203.1 1.6 copy_convert_fusion
  204.7 0.5 copy-done.4
  205.1 1.9 copy.67
  207.1 8.0 %add_convert_fusion = bf16[1,1024,512]{2,1,0:T(8,128)(2,1)S(1)} fusion(f32[1,1024,512]{2,1,0:T(8,128)S(1)} %bitcast.163, f32[512]{0:T(512)S(1)} %bitcast.210, f32[512]{0:T(512)S(1)} %bitcast.212, f32[512]{0:T(512)S(1)} %bitcast.216, f32[512]{0:T(512)S(1)} %bitcast.218, f32[512]{0:T(512)S(1)} %bitcast.220, f32[512]{0:T(512)S(1)} %bitcast.222, ...), kind=kLoop, calls=%fused_computation.52 | loop fusion | flops 32505856 | bytes 3209216 | tf_op jit(solution)/shard_map/convert_element_type | solution.py:59
  215.0 2.9 copy.88
  218.0 8.0 %reduce.21 = bf16[1024,512]{1,0:T(8,128)(2,1)S(1)} reduce(bf16[1024,1,512]{2,1,0:T(2,128)(2,1)} %bitcast.180, bf16[]{:T(256)} %broadcast.201), dimensions={1}, to_apply=%bitcast.160.reduce_sub_computation | reduce | bytes 2097154
  226.0 2.0 reshape.399
  228.0 4.1 %all-to-all-start.3 = ((bf16[4,2,65536]{2,1,0:T(2,128)(2,1)}), bf16[4,2,65536]{2,1,0:T(2,128)(2,1)S(1)}, u32[]{:S(2)}, u32[]{:S(2)}) async-start(bf16[4,2,65536]{2,1,0:T(2,128)(2,1)} %reshape.399), calls=%async_computation.3 | async-start | bytes 2097152 | tf_op jit(solution)/shard_map/all_to_all | solution.py:58
  232.1 0.2 all-reduce.4.cloned.1.call-start
  232.3 17.9 %multiply_reduce_fusion.2 = (f32[512]{0:T(512)S(1)}, f32[512]{0:T(512)S(1)}, f32[512]{0:T(512)S(1)}, f32[512]{0:T(512)S(1)}, f32[512]{0:T(512)S(1)}, /*index=5*/...) fusion(f32[1,1024,512]{2,1,0:T(8,128)} %bitcast.165, ...), kind=kLoop, calls=%fused_computation.22 | loop fusion | flops 18865152 | bytes 4231168 | tf_op jit(solution)/shard_map/reduce_sum | solution.py:56
  250.2 46.1 %reduce-scatter.2.cloned.1.call-done = f32[256,2048]{0,1:T(8,128)} async-done(((f32[2048,2048]{0,1:T(8,128)}), f32[256,2048]{0,1:T(8,128)}) %reduce-scatter.2.cloned.1.call-update) | async-done | bytes 2097168 | tf_op jit(solution)/shard_map/reduce_scatter | solution.py:65
  296.3 2.6 multiply_reduce_fusion.1
  298.9 11.8 %multiply_reduce_fusion.3 = (f32[512]{0:T(512)S(1)}, f32[512]{0:T(512)S(1)}, f32[512]{0:T(512)S(1)}, f32[512]{0:T(512)S(1)}, f32[512]{0:T(512)S(1)}, /*index=5*/...) fusion(f32[1,1024,512]{2,1,0:T(8,128)} %bitcast.166, ...), kind=kLoop, calls=%fused_computation.23 | loop fusion | flops 12576768 | bytes 4218880 | tf_op jit(solution)/shard_map/reduce_sum | solution.py:56
  310.7 0.1 stack.127
  310.9 14.8 %all-gather.1 = f32[8,31,512]{2,1,0:T(8,128)S(1)} all-gather(f32[1,31,512]{2,1,0:T(8,128)S(1)} %bitcast.188), channel_id=2, replica_groups=mesh['sp'=4,'dp'=8] {'dp'}, dimensions={0}, use_global_device_ids=true | all-gather | bytes 571392 | tf_op jit(solution)/shard_map/all_gather | solution.py:57
  325.7 0.7 reduce_sum.386
  326.4 0.9 reshape.400
  327.3 0.3 copy.69
  327.6 1.6 convert_bitcast_fusion
  329.3 3.0 copy.70
  332.3 3.4 fusion.4
  335.7 2.3 copy.72
  337.9 1.4 copy.73
  339.4 28.0 %all-reduce.4.cloned.1.call-done = f32[256,2048]{0,1:T(8,128)} async-done(((f32[256,2048]{0,1:T(8,128)}), f32[256,2048]{0,1:T(8,128)}) %all-reduce.4.cloned.1.call-update) | async-done | bytes 2097168 | tf_op jit(solution)/shard_map/psum | solution.py:73
  367.4 2.9 copy.74
  (38 shorter events, 0.3 us)
Async XLA Ops:
  7.2 110.3 %copy-start = (bf16[1,256,2048]{2,1,0:T(8,128)(2,1)S(1)}, bf16[1,256,2048]{2,1,0:T(8,128)(2,1)}, u32[]{:S(2)}) copy-start(bf16[1,256,2048]{2,1,0:T(8,128)(2,1)} %param.8) | copy-start | bytes 3145732
  7.2 121.8 %all-gather.4.cloned.1.call-start = ((), (), s32[]{:S(2)}) async-start(), calls=%async_computation.5 | async-start | bytes 9437184 | tf_op jit(solution)/shard_map/all_gather | solution.py:36
  9.4 2.5 copy-start.6
  11.3 13.5 %copy-start.8 = (bf16[1,256,2048]{1,2,0:T(8,128)(2,1)}, bf16[1,256,2048]{1,2,0:T(8,128)(2,1)S(1)}, u32[]{:S(2)}) copy-start(bf16[1,256,2048]{1,2,0:T(8,128)(2,1)S(1)} %copy.57) | copy-start | bytes 3145732
  37.0 7.0 %copy-start.10 = (f32[31,512]{1,0:T(8,128)S(1)}, f32[31,512]{1,0:T(8,128)}, u32[]{:S(2)}) copy-start(f32[31,512]{1,0:T(8,128)} %param.9) | copy-start | bytes 190468
  38.6 19.7 %all-to-all-start = ((bf16[4,2,65536]{2,1,0:T(2,128)(2,1)}), bf16[4,2,65536]{2,1,0:T(2,128)(2,1)}, u32[]{:S(2)}, u32[]{:S(2)}) async-start(bf16[4,2,65536]{2,1,0:T(2,128)(2,1)} %reshape.393), calls=%async_computation | async-start | bytes 2097152 | tf_op jit(solution)/shard_map/all_to_all | solution.py:14
  60.9 2.0 copy-start.3
  64.9 10.9 %copy-start.2 = (f32[1,4,256,512]{3,2,1,0:T(8,128)}, f32[1,4,256,512]{3,2,1,0:T(8,128)S(1)}, u32[]{:S(2)}) copy-start(f32[1,4,256,512]{3,2,1,0:T(8,128)S(1)} %copy.60) | copy-start | bytes 6291460
  83.9 6.3 %copy-start.11 = (f32[2048]{0:T(1024)S(1)}, f32[2048]{0:T(1024)}, u32[]{:S(2)}) copy-start(f32[2048]{0:T(1024)} %param.10) | copy-start | bytes 24580
  85.9 17.7 %all-to-all-start.1 = ((bf16[4,2,65536]{2,1,0:T(2,128)(2,1)}), bf16[4,2,65536]{2,1,0:T(2,128)(2,1)}, u32[]{:S(2)}, u32[]{:S(2)}) async-start(bf16[4,2,65536]{2,1,0:T(2,128)(2,1)} %reshape.395), calls=%async_computation.1 | async-start | bytes 2097152 | tf_op jit(solution)/shard_map/all_to_all | solution.py:22
  90.2 206.1 %reduce-scatter.2.cloned.1.call-start = ((), (), s32[]{:S(2)}) async-start(), calls=%async_computation.6 | async-start | bytes 18874368 | tf_op jit(solution)/shard_map/reduce_scatter | solution.py:65
  106.4 1.3 copy-start.5
  149.8 52.3 %all-to-all-start.2 = ((bf16[4,2,65536]{2,1,0:T(2,128)(2,1)}), bf16[4,2,65536]{2,1,0:T(2,128)(2,1)S(1)}, u32[]{:S(2)}, u32[]{:S(2)}) async-start(bf16[4,2,65536]{2,1,0:T(2,128)(2,1)} %reshape.397), calls=%async_computation.2 | async-start | bytes 2097152 | tf_op jit(solution)/shard_map/all_to_all | solution.py:47
  203.1 2.0 copy-start.4
  228.0 98.4 %all-to-all-start.3 = ((bf16[4,2,65536]{2,1,0:T(2,128)(2,1)}), bf16[4,2,65536]{2,1,0:T(2,128)(2,1)S(1)}, u32[]{:S(2)}, u32[]{:S(2)}) async-start(bf16[4,2,65536]{2,1,0:T(2,128)(2,1)} %reshape.399), calls=%async_computation.3 | async-start | bytes 2097152 | tf_op jit(solution)/shard_map/all_to_all | solution.py:58
  232.1 135.3 %all-reduce.4.cloned.1.call-start = ((), (), s32[]{:S(2)}) async-start(), calls=%async_computation.7 | async-start | bytes 4194304 | tf_op jit(solution)/shard_map/psum | solution.py:73
  329.2 3.1 copy-start.7
  329.2 3.1 copy-start.9
  337.9 32.3 %copy-start.1 = (bf16[1,256,2048]{2,1,0:T(8,128)(2,1)S(1)}, bf16[1,256,2048]{2,1,0:T(8,128)(2,1)}, u32[]{:S(2)}) copy-start(bf16[1,256,2048]{2,1,0:T(8,128)(2,1)} %param.8) | copy-start | bytes 3145732
Sparse Core Ops, SparseCore 0:
  9.6 84.7 all-gather.3
  126.9 169.3 reduce-scatter.1
  299.4 67.9 all-reduce.3
